TPU v7x, 32 devices: a whole 2x2x4 slice. The times are simulated.
32 devices in a mesh: grp: 2 (over y), fs: 4 (over z), tp: 4 (over x, core).
Axes of the slice: x: 2, y: 2, z: 4, core: 2. Of those that a mesh axis runs over, the one named last changes fastest.
Arguments:
- tokens: bfloat16 [8, 384, 2048], P(('grp', 'fs'), None, 'tp'), parts along dimension 0, may hold values from -24 to 24
- input_gain: float32 [2048], replicated, may hold values from 0.1 to 1.9
- query_weight: bfloat16 [2048, 1024], P('fs', 'tp'), may hold values from -0.125 to 0.125
- key_weight: bfloat16 [2048, 1024], P('fs', 'tp'), may hold values from -0.125 to 0.125
- value_weight: bfloat16 [2048, 1024], P('fs', 'tp'), may hold values from -0.125 to 0.125
- output_gate_matrix: bfloat16 [2048, 1024], P('fs', 'tp'), may hold values from -0.125 to 0.125
- forward_decay: float32 [16], P('tp'), may hold values from -1 to 9
- backward_decay: float32 [16], P('tp'), may hold values from -1 to 9
- merge_weight: bfloat16 [1024, 2048], P('tp', 'fs'), may hold values from -0.375 to 0.375
- middle_gain: float32 [2048], replicated, may hold values from 0.1 to 1.9
- gate_weight: bfloat16 [2048, 5120], P('fs', 'tp'), may hold values from -0.125 to 0.125
- up_weight: bfloat16 [2048, 5120], P('fs', 'tp'), may hold values from -0.125 to 0.125
- down_weight: bfloat16 [5120, 2048], P('tp', 'fs'), may hold values from -0.15625 to 0.15625
Outputs:
- layer_out: bfloat16 [8, 384, 2048], P(('grp', 'fs'), None, 'tp'), parts along dimension 0
There are 2 independent parts, one for each index of `grp`. A program takes and returns all parts, laid end to end along the dimension named above; an argument that names none is the same for every part. Nothing has to cross between parts.
All inputs are finite; a program needn't handle non-finite values.
Results may differ from a plain program's by a relative error of at most 0.019.
Values may be sent and summed in bfloat16 or wider, within the bound.
A program may use at most 64 MiB of HBM per device.

v0:
```python
import jax
import jax.numpy as jnp
from jax import lax
from jax.sharding import PartitionSpec as P

BLOCK = 128
norm_eps = 1e-06
group_eps = 1e-05
rope_base = 10000.0
highest_precision = lax.Precision.HIGHEST


def rms_scale(values, gain_vector):
    widened = values.astype(jnp.float32)
    scaled = widened * lax.rsqrt(jnp.mean(widened * widened, axis=-1, keepdims=True) + norm_eps)
    return (scaled * gain_vector).astype(jnp.bfloat16)


def apply_rotary_heads(values, length):
    half_dim = values.shape[-1] // 2
    inverse = rope_base ** (-jnp.arange(half_dim, dtype=jnp.float32) / half_dim)
    angles = jnp.arange(length, dtype=jnp.float32)[:, None] * inverse[None, :]
    cosine = jnp.cos(angles)[:, None, :]
    sine_part = jnp.sin(angles)[:, None, :]
    lower_half = values[..., :half_dim]
    upper_half = values[..., half_dim:]
    return jnp.concatenate(
        [
            lower_half * cosine - upper_half * sine_part,
            upper_half * cosine + lower_half * sine_part,
        ],
        axis=-1,
    )


def carry_states(key_blocks, value_blocks, weighting, log_rates, block_size, backward):
    block_terms = jnp.einsum(
        "sbmhd,sbmhe->bshde",
        key_blocks * weighting[None, None, :, :, None],
        value_blocks,
        precision=highest_precision,
    )
    factor = jnp.exp(log_rates * block_size)[None, :, None, None]

    def advance(running, addend):
        return (running * factor + addend, running)

    initial = jnp.zeros(block_terms.shape[1:], jnp.float32)
    return lax.scan(advance, initial, block_terms, reverse=backward)[1]


def retain_blocks(
    query_rows, key_rows, value_rows, gate_rows, forward_decay, backward_decay, seq_count, length
):
    head_count = forward_decay.shape[0]
    head_dim = query_rows.shape[1] // head_count
    block_size = BLOCK
    block_count = length // block_size

    def split_heads(rows_in):
        return rows_in.astype(jnp.float32).reshape(seq_count, length, head_count, head_dim)

    def blocked(tensor):
        return tensor.reshape(seq_count, block_count, block_size, head_count, head_dim)

    queries = blocked(apply_rotary_heads(split_heads(query_rows), length))
    key_heads = blocked(apply_rotary_heads(split_heads(key_rows), length) * head_dim ** (-0.5))
    valued = blocked(split_heads(value_rows))
    rate_ahead = jax.nn.log_sigmoid(forward_decay)
    rate_behind = jax.nn.log_sigmoid(backward_decay)
    position = jnp.arange(block_size, dtype=jnp.float32)
    offset = position[:, None] - position[None, :]
    inside = jnp.where(
        offset[None] >= 0,
        jnp.exp(rate_ahead[:, None, None] * jnp.maximum(offset, 0.0)[None]),
        jnp.exp(rate_behind[:, None, None] * jnp.maximum(-offset, 0.0)[None]),
    )
    attention_scores = (
        jnp.einsum("sbchd,sbmhd->sbhcm", queries, key_heads, precision=highest_precision)
        * inside[None, None]
    )
    result = jnp.einsum("sbhcm,sbmhd->sbchd", attention_scores, valued, precision=highest_precision)
    column = position[:, None]
    key_ahead = jnp.exp(rate_ahead[None, :] * (block_size - 1 - column))
    query_ahead = jnp.exp(rate_ahead[None, :] * (column + 1))
    key_behind = jnp.exp(rate_behind[None, :] * column)
    query_behind = jnp.exp(rate_behind[None, :] * (block_size - column))
    from_before = carry_states(key_heads, valued, key_ahead, rate_ahead, block_size, False)
    from_after = carry_states(key_heads, valued, key_behind, rate_behind, block_size, True)
    result = (
        result
        + jnp.einsum("sbchd,bshde->sbche", queries, from_before, precision=highest_precision)
        * query_ahead[None, None, :, :, None]
    )
    result = (
        result
        + jnp.einsum("sbchd,bshde->sbche", queries, from_after, precision=highest_precision)
        * query_behind[None, None, :, :, None]
    )
    result = result.reshape(seq_count, length, head_count, head_dim)
    center = jnp.mean(result, axis=-1, keepdims=True)
    spread = jnp.mean(jnp.square(result - center), axis=-1, keepdims=True)
    normalized = (result - center) * lax.rsqrt(spread + group_eps)
    gated = jax.nn.silu(split_heads(gate_rows)) * normalized
    return gated.reshape(seq_count * length, head_count * head_dim).astype(jnp.bfloat16)


def accumulate(pieces, source):
    return tuple(
        (
            jnp.dot(source, weight_piece, preferred_element_type=jnp.float32)
            for weight_piece in pieces
        )
    )


def on_device(
    tokens,
    input_gain,
    query_weight,
    key_weight,
    value_weight,
    output_gate_matrix,
    forward_decay,
    backward_decay,
    merge_weight,
    middle_gain,
    gate_weight,
    up_weight,
    down_weight,
):
    seq_count, length, part_width = tokens.shape
    row_count = seq_count * length
    gathered = lax.all_gather(tokens, "tp", axis=2, tiled=True)
    normed = rms_scale(gathered.reshape(row_count, gathered.shape[2]), input_gain)
    query_sum, key_sum, value_sum, gating_sum = accumulate(
        (
            lax.all_gather(query_weight, "fs", axis=0, tiled=True),
            lax.all_gather(key_weight, "fs", axis=0, tiled=True),
            lax.all_gather(value_weight, "fs", axis=0, tiled=True),
            lax.all_gather(output_gate_matrix, "fs", axis=0, tiled=True),
        ),
        normed,
    )
    mixed = retain_blocks(
        query_sum.astype(jnp.bfloat16),
        key_sum.astype(jnp.bfloat16),
        value_sum.astype(jnp.bfloat16),
        gating_sum.astype(jnp.bfloat16),
        forward_decay,
        backward_decay,
        seq_count,
        length,
    )
    merge_term = jnp.dot(
        mixed,
        lax.all_gather(merge_weight, "fs", axis=1, tiled=True),
        preferred_element_type=jnp.float32,
    )
    merged = lax.psum_scatter(
        merge_term.astype(jnp.bfloat16), "tp", scatter_dimension=1, tiled=True
    ).astype(jnp.float32)
    middle = (tokens.reshape(row_count, part_width).astype(jnp.float32) + merged).astype(
        jnp.bfloat16
    )
    gathered_mid = lax.all_gather(middle, "tp", axis=1, tiled=True)
    normed_mid = rms_scale(gathered_mid, middle_gain)
    gate_full, up_full = (
        lax.all_gather(gate_weight, "fs", axis=0, tiled=True),
        lax.all_gather(up_weight, "fs", axis=0, tiled=True),
    )
    gate_act = jnp.dot(normed_mid, gate_full, preferred_element_type=jnp.float32)
    up_act = jnp.dot(normed_mid, up_full, preferred_element_type=jnp.float32)
    hidden = (jax.nn.silu(gate_act) * up_act).astype(jnp.bfloat16)
    down_term = jnp.dot(
        hidden,
        lax.all_gather(down_weight, "fs", axis=1, tiled=True),
        preferred_element_type=jnp.float32,
    )
    summed = lax.psum_scatter(
        down_term.astype(jnp.bfloat16), "tp", scatter_dimension=1, tiled=True
    ).astype(jnp.float32)
    layer_out = (middle.astype(jnp.float32) + summed).astype(jnp.bfloat16)
    return layer_out.reshape(seq_count, length, part_width)


def solution(mesh):
    placed = (
        P(("grp", "fs"), None, "tp"),
        P(),
        P("fs", "tp"),
        P("fs", "tp"),
        P("fs", "tp"),
        P("fs", "tp"),
        P("tp"),
        P("tp"),
        P("tp", "fs"),
        P(),
        P("fs", "tp"),
        P("fs", "tp"),
        P("tp", "fs"),
    )
    return jax.shard_map(
        on_device,
        mesh=mesh,
        in_specs=placed,
        out_specs=P(("grp", "fs"), None, "tp"),
        check_vma=False,
    )
```

profile of v0, /device:TPU:0, one launch (start us, length us, event | category | flops | bytes accessed | tf_op | source)
XLA Modules:
  0.0 571.5 jit_solution(758774433648440747)
XLA Ops:
  6.5 0.7 all-gather.11.cloned.1.call-update
  13.1 18.2 %all-gather.11.cloned.1.call-done = bf16[1,384,2048]{2,1,0:T(8,128)(2,1)} async-done(((bf16[1,384,512]{2,1,0:T(8,128)(2,1)}), bf16[1,384,2048]{2,1,0:T(8,128)(2,1)}) %all-gather.11.cloned.1.call-update) | async-done | bytes 1572880 | tf_op jit(solution)/shard_map/all_gather | solution.py:134
  31.3 1.9 fusion.3
  33.2 27.7 %all-gather.17.cloned.1.call-done = bf16[2048,256]{1,0:T(8,128)(2,1)} async-done(((bf16[512,256]{1,0:T(8,128)(2,1)}), bf16[2048,256]{1,0:T(8,128)(2,1)}) %all-gather.17.cloned.1.call-update) | async-done | bytes 1048592 | tf_op jit(solution)/shard_map/all_gather | solution.py:138
  60.9 2.6 convolution_convert_fusion.3
  63.5 26.4 %all-gather.19.cloned.1.call-done = bf16[2048,256]{1,0:T(8,128)(2,1)} async-done(((bf16[512,256]{1,0:T(8,128)(2,1)}), bf16[2048,256]{1,0:T(8,128)(2,1)}) %all-gather.19.cloned.1.call-update) | async-done | bytes 1048592 | tf_op jit(solution)/shard_map/all_gather | solution.py:139
  89.8 2.1 convolution_convert_fusion.2
  92.0 0.9 multiply_subtract_fusion.1
  93.0 1.7 concatenate.22
  94.7 1.0 pad_maximum_fusion
  96.0 22.7 %all-gather.15.cloned.1.call-done = bf16[2048,256]{1,0:T(8,128)(2,1)} async-done(((bf16[512,256]{1,0:T(8,128)(2,1)}), bf16[2048,256]{1,0:T(8,128)(2,1)}) %all-gather.15.cloned.1.call-update) | async-done | bytes 1048592 | tf_op jit(solution)/shard_map/all_gather | solution.py:140
  118.6 2.6 convolution_convert_fusion.4
  121.2 1.2 reshape.432
  124.7 0.8 fusion.9
  125.5 0.8 fusion.10
  126.3 1.4 convolution_multiply_fusion.1
  127.8 0.9 fusion.43
  129.0 1.2 reshape.431
  130.8 16.7 %all-gather.13.cloned.1.call-done = bf16[2048,256]{1,0:T(8,128)(2,1)} async-done(((bf16[512,256]{1,0:T(8,128)(2,1)}), bf16[2048,256]{1,0:T(8,128)(2,1)}) %all-gather.13.cloned.1.call-update) | async-done | bytes 1048592 | tf_op jit(solution)/shard_map/all_gather | solution.py:141
  147.4 28.8 %all-gather.21.cloned.1.call-done = bf16[256,2048]{1,0:T(8,128)(2,1)} async-done(((bf16[256,512]{1,0:T(8,128)(2,1)}), bf16[256,2048]{1,0:T(8,128)(2,1)}) %all-gather.21.cloned.1.call-update) | async-done | bytes 1048592 | tf_op jit(solution)/shard_map/all_gather | solution.py:157
  176.3 4.7 convolution_convert_fusion.1
  181.1 27.5 %reduce-scatter.3.cloned.1.call-done = bf16[384,512]{1,0:T(8,128)(2,1)} async-done(((bf16[384,2048]{1,0:T(8,128)(2,1)}), bf16[384,512]{1,0:T(8,128)(2,1)}) %reduce-scatter.3.cloned.1.call-update) | async-done | bytes 393232 | tf_op jit(solution)/shard_map/reduce_scatter | solution.py:160
  208.5 1.8 fusion.12
  212.7 17.5 %all-gather.23.cloned.1.call-done = bf16[384,2048]{1,0:T(8,128)(2,1)} async-done(((bf16[384,512]{1,0:T(8,128)(2,1)}), bf16[384,2048]{1,0:T(8,128)(2,1)}) %all-gather.23.cloned.1.call-update) | async-done | bytes 1572880 | tf_op jit(solution)/shard_map/all_gather | solution.py:166
  230.2 1.8 fusion
  232.0 97.8 %all-gather.25.cloned.1.call-done = bf16[2048,1280]{1,0:T(8,128)(2,1)} async-done(((bf16[512,1280]{1,0:T(8,128)(2,1)}), bf16[2048,1280]{1,0:T(8,128)(2,1)}) %all-gather.25.cloned.1.call-update) | async-done | bytes 5242896 | tf_op jit(solution)/shard_map/all_gather | solution.py:169
  329.8 6.5 %fusion.15 = f32[384,1280]{1,0:T(8,128)} fusion(bf16[2048,1280]{1,0:T(8,128)(2,1)} %all-gather.25.cloned.1.call-done, bf16[384,2048]{1,0:T(8,128)(2,1)} %all-gather.23.cloned.1.call-done, f32[2048]{0:T(1024)S(1)} %copy-done.12, f32[384]{0:T(512)S(1)} %add_rsqrt_fusion), kind=kOutput, calls=%fused_computation.36 | convolution fusion | flops 2016411648 | bytes 8791552 | tf_op jit(solution)/shard_map/dot_general | solution.py:172
  336.4 91.3 %all-gather.27.cloned.1.call-done = bf16[2048,1280]{1,0:T(8,128)(2,1)} async-done(((bf16[512,1280]{1,0:T(8,128)(2,1)}), bf16[2048,1280]{1,0:T(8,128)(2,1)}) %all-gather.27.cloned.1.call-update) | async-done | bytes 5242896 | tf_op jit(solution)/shard_map/all_gather | solution.py:170
  427.7 98.0 %all-gather.29.cloned.1.call-done = bf16[1280,2048]{1,0:T(8,128)(2,1)} async-done(((bf16[1280,512]{1,0:T(8,128)(2,1)}), bf16[1280,2048]{1,0:T(8,128)(2,1)}) %all-gather.29.cloned.1.call-update) | async-done | bytes 5242896 | tf_op jit(solution)/shard_map/all_gather | solution.py:177
  525.6 10.7 %convolution_convert_fusion = bf16[384,2048]{1,0:T(8,128)(2,1)} fusion(bf16[1280,2048]{1,0:T(8,128)(2,1)} %all-gather.29.cloned.1.call-done, bf16[2048,1280]{1,0:T(8,128)(2,1)} %all-gather.27.cloned.1.call-done, f32[384,1280]{1,0:T(8,128)} %fusion.15, bf16[384,2048]{1,0:T(8,128)(2,1)S(1)} %copy-done.3, f32[2048]{0:T(1024)S(1)} %copy-done.12, ...), kind=kOutput, calls=%fused_computation.15 | convolution fusion | flops 4033413120 | bytes 15607296 | tf_op jit(solution)/shard_map/dot_general | solution.py:175
  536.3 26.5 %reduce-scatter.5.cloned.1.call-done = bf16[384,512]{1,0:T(8,128)(2,1)} async-done(((bf16[384,2048]{1,0:T(8,128)(2,1)}), bf16[384,512]{1,0:T(8,128)(2,1)}) %reduce-scatter.5.cloned.1.call-update) | async-done | bytes 393232 | tf_op jit(solution)/shard_map/reduce_scatter | solution.py:180
  562.8 1.8 fusion.17
  (97 shorter events, 12.1 us)
Async XLA Ops:
  6.5 54.3 %copy-start.10 = (f32[2048]{0:T(1024)S(1)}, f32[2048]{0:T(1024)}, u32[]{:S(2)}) copy-start(f32[2048]{0:T(1024)} %param.18) | copy-start | bytes 24580
  6.5 24.7 %all-gather.11.cloned.1.call-start = ((), (), s32[]{:S(2)}) async-start(), calls=%async_computation.2 | async-start | bytes 1966080 | tf_op jit(solution)/shard_map/all_gather | solution.py:134
  7.3 53.6 %all-gather.17.cloned.1.call-start = ((), (), s32[]{:S(2)}) async-start(), calls=%async_computation.5 | async-start | bytes 1310720 | tf_op jit(solution)/shard_map/all_gather | solution.py:138
  8.0 81.8 %all-gather.19.cloned.1.call-start = ((), (), s32[]{:S(2)}) async-start(), calls=%async_computation.6 | async-start | bytes 1310720 | tf_op jit(solution)/shard_map/all_gather | solution.py:139
  8.7 109.9 %all-gather.15.cloned.1.call-start = ((), (), s32[]{:S(2)}) async-start(), calls=%async_computation.4 | async-start | bytes 1310720 | tf_op jit(solution)/shard_map/all_gather | solution.py:140
  9.3 138.1 %all-gather.13.cloned.1.call-start = ((), (), s32[]{:S(2)}) async-start(), calls=%async_computation.3 | async-start | bytes 1310720 | tf_op jit(solution)/shard_map/all_gather | solution.py:141
  9.9 166.4 %all-gather.21.cloned.1.call-start = ((), (), s32[]{:S(2)}) async-start(), calls=%async_computation.7 | async-start | bytes 1310720 | tf_op jit(solution)/shard_map/all_gather | solution.py:157
  10.5 198.1 %reduce-scatter.3.cloned.1.call-start = ((), (), s32[]{:S(2)}) async-start(), calls=%async_computation.8 | async-start | bytes 1966080 | tf_op jit(solution)/shard_map/reduce_scatter | solution.py:160
  31.3 58.6 %copy-start.1 = (bf16[1,384,2048]{2,1,0:T(8,128)(2,1)S(1)}, bf16[1,384,2048]{2,1,0:T(8,128)(2,1)}, u32[]{:S(2)}) copy-start(bf16[1,384,2048]{2,1,0:T(8,128)(2,1)} %all-gather.11.cloned.1.call-done) | copy-start | bytes 4718596
  33.2 58.7 %copy-start.8 = (f32[384]{0:T(512)}, f32[384]{0:T(512)S(1)}, u32[]{:S(2)}) copy-start(f32[384]{0:T(512)S(1)} %add_rsqrt_fusion.1) | copy-start | bytes 4612
  95.9 26.7 %copy-start.5 = (f32[3,128,4,32]{1,0,3,2:T(4,128)S(1)}, f32[3,128,4,32]{1,0,3,2:T(4,128)}, u32[]{:S(2)}) copy-start(f32[3,128,4,32]{1,0,3,2:T(4,128)} %concatenate.22) | copy-start | bytes 589828
  95.9 26.7 %copy-start.6 = (f32[128,4]{0,1:T(4,128)S(1)}, f32[128,4]{0,1:T(4,128)}, u32[]{:S(2)}) copy-start(f32[128,4]{0,1:T(4,128)} %get-tuple-element.231) | copy-start | bytes 6148
  95.9 26.7 %copy-start.7 = (f32[128,4]{0,1:T(4,128)S(1)}, f32[128,4]{0,1:T(4,128)}, u32[]{:S(2)}) copy-start(f32[128,4]{0,1:T(4,128)} %get-tuple-element.229) | copy-start | bytes 6148
  127.8 48.5 %copy-start.2 = (bf16[1,384,2048]{2,1,0:T(8,128)(2,1)S(1)}, bf16[1,384,2048]{2,1,0:T(8,128)(2,1)}, u32[]{:S(2)}) copy-start(bf16[1,384,2048]{2,1,0:T(8,128)(2,1)} %all-gather.11.cloned.1.call-done) | copy-start | bytes 4718596
  127.8 48.5 %copy-start.9 = (f32[384]{0:T(512)S(1)}, f32[384]{0:T(512)}, u32[]{:S(2)}) copy-start(f32[384]{0:T(512)} %copy-done.8) | copy-start | bytes 4612
  127.8 48.5 %copy-start.11 = (f32[2048]{0:T(1024)S(1)}, f32[2048]{0:T(1024)}, u32[]{:S(2)}) copy-start(f32[2048]{0:T(1024)} %param.18) | copy-start | bytes 24580
  130.7 77.8 %copy-start.4 = (bf16[1,384,512]{2,1,0:T(8,128)(2,1)S(1)}, bf16[1,384,512]{2,1,0:T(8,128)(2,1)}, u32[]{:S(2)}) copy-start(bf16[1,384,512]{2,1,0:T(8,128)(2,1)} %param.17) | copy-start | bytes 1179652
  181.0 49.2 %all-gather.23.cloned.1.call-start = ((), (), s32[]{:S(2)}) async-start(), calls=%async_computation.9 | async-start | bytes 1966080 | tf_op jit(solution)/shard_map/all_gather | solution.py:166
  210.4 119.5 %copy-start.12 = (f32[2048]{0:T(1024)S(1)}, f32[2048]{0:T(1024)}, u32[]{:S(2)}) copy-start(f32[2048]{0:T(1024)} %param.26) | copy-start | bytes 24580
  210.4 119.4 %all-gather.25.cloned.1.call-start = ((), (), s32[]{:S(2)}) async-start(), calls=%async_computation.10 | async-start | bytes 6553600 | tf_op jit(solution)/shard_map/all_gather | solution.py:169
  211.1 216.5 %all-gather.27.cloned.1.call-start = ((), (), s32[]{:S(2)}) async-start(), calls=%async_computation.11 | async-start | bytes 6553600 | tf_op jit(solution)/shard_map/all_gather | solution.py:170
  211.7 313.9 %all-gather.29.cloned.1.call-start = ((), (), s32[]{:S(2)}) async-start(), calls=%async_computation.12 | async-start | bytes 6553600 | tf_op jit(solution)/shard_map/all_gather | solution.py:177
  212.5 350.4 %reduce-scatter.5.cloned.1.call-start = ((), (), s32[]{:S(2)}) async-start(), calls=%async_computation.13 | async-start | bytes 1966080 | tf_op jit(solution)/shard_map/reduce_scatter | solution.py:180
  232.0 293.6 %copy-start.3 = (bf16[384,2048]{1,0:T(8,128)(2,1)S(1)}, bf16[384,2048]{1,0:T(8,128)(2,1)}, u32[]{:S(2)}) copy-start(bf16[384,2048]{1,0:T(8,128)(2,1)} %all-gather.23.cloned.1.call-done) | copy-start | bytes 4718596
  336.4 226.4 %copy-start = (bf16[384,512]{1,0:T(8,128)(2,1)S(1)}, bf16[384,512]{1,0:T(8,128)(2,1)}, u32[]{:S(2)}) copy-start(bf16[384,512]{1,0:T(8,128)(2,1)} %fusion.12) | copy-start | bytes 1179652
Sparse Core Ops, SparseCore 0:
  8.9 22.3 all-gather.10
  32.8 27.9 all-gather.16
  62.4 27.3 all-gather.18
  91.3 27.3 all-gather.14
  120.1 27.3 all-gather.12
  148.9 27.3 all-gather.20
  181.1 27.3 reduce-scatter.2
  210.5 19.6 all-gather.22
  231.8 98.0 all-gather.24
  331.3 96.3 all-gather.26
  429.2 96.3 all-gather.28
  536.5 26.3 reduce-scatter.4
where the time goes:
time: 572 us; the launch traced here: 571 us
  waiting for transfers between devices  505 us (88%)
  matrix products  33.9 us (6%)
  between operations  13.9 us (2%)
  other arithmetic  12.9 us (2%)
    all_gather x1, waiting for transfers between devices, on_device(): lax.all_gather(down_weight, 'fs', axis=1, tiled=True)  98 us
    all_gather x1, waiting for transfers between devices, on_device(): lax.all_gather(gate_weight, 'fs', axis=0, tiled=True)  97.8 us
    all_gather x1, waiting for transfers between devices, on_device(): lax.all_gather(up_weight, 'fs', axis=0, tiled=True)  91.3 us
    all_gather x1, waiting for transfers between devices, on_device(): lax.all_gather(merge_weight, 'fs', axis=1, tiled=True)  28.8 us
    all_gather x1, waiting for transfers between devices, on_device(): lax.all_gather(query_weight, 'fs', axis=0, tiled=True)  27.7 us
    reduce_scatter x1, waiting for transfers between devices, on_device(): lax.psum_scatter(merge_term.astype(jnp.bfloat16), 'tp', scatter_dimension...  27.5 us
    reduce_scatter x1, waiting for transfers between devices, on_device(): lax.psum_scatter(down_term.astype(jnp.bfloat16), 'tp', scatter_dimension=...  26.5 us
    all_gather x1, waiting for transfers between devices, on_device(): lax.all_gather(key_weight, 'fs', axis=0, tiled=True)  26.4 us
  transfers between devices with their start and end apart: 12, of which 12 were waited for; matrix products, arithmetic and copies ran while one was open for 6% of the time, Pallas kernels for 0%

commit v1 on v0

--- a/solution.py
+++ b/solution.py
@@ -8,6 +8,19 @@
 group_eps = 1e-05
 rope_base = 10000.0
 highest_precision = lax.Precision.HIGHEST
+
+
+def collect(x, axis, dim):
+    ways = lax.axis_size(axis)
+    up = [(d, (d + 1) % ways) for d in range(ways)]
+    down = [(d, (d - 1) % ways) for d in range(ways)]
+    earlier, later = ([x], [x])
+    for _ in range(ways // 2):
+        earlier.append(lax.ppermute(earlier[-1], axis, up))
+    for _ in range((ways - 1) // 2):
+        later.append(lax.ppermute(later[-1], axis, down))
+    line = jnp.concatenate([*earlier[::-1], *later[1:]], axis=dim)
+    return jnp.roll(line, (lax.axis_index(axis) - ways // 2) * x.shape[dim], axis=dim)
 
 
 def rms_scale(values, gain_vector):
@@ -172,11 +185,7 @@
     gate_act = jnp.dot(normed_mid, gate_full, preferred_element_type=jnp.float32)
     up_act = jnp.dot(normed_mid, up_full, preferred_element_type=jnp.float32)
     hidden = (jax.nn.silu(gate_act) * up_act).astype(jnp.bfloat16)
-    down_term = jnp.dot(
-        hidden,
-        lax.all_gather(down_weight, "fs", axis=1, tiled=True),
-        preferred_element_type=jnp.float32,
-    )
+    down_term = jnp.dot(hidden, collect(down_weight, "fs", 1), preferred_element_type=jnp.float32)
     summed = lax.psum_scatter(
         down_term.astype(jnp.bfloat16), "tp", scatter_dimension=1, tiled=True
     ).astype(jnp.float32)

time: 572 us -> 529 us (0.925)
  waiting for transfers between devices: 505 us -> 449 us
  local copies, waits for them, and re-layouts: 5.47 us -> 17.1 us
    ppermute x0 -> x3, waiting for transfers between devices: none -> 138 us  [the longest x2 88.6 us: collect(): earlier.append(lax.ppermute(earlier[-1], axis, up))]
    all_gather x1 -> x0, waiting for transfers between devices: 98 us -> none  [on_device(): lax.all_gather(down_weight, 'fs', axis=1, tiled=True)]
    all_gather x1, waiting for transfers between devices: 97.8 us -> 13.9 us  [on_device(): lax.all_gather(gate_weight, 'fs', axis=0, tiled=True)]
    all_gather x1, waiting for transfers between devices: 17.5 us -> 0.01 us  [on_device(): gathered_mid = lax.all_gather(middle, 'tp', axis=1, tiled=True)]
    unnamed x27 -> x24, local copies, waits for them, and re-layouts: 0.1 us -> 12.6 us
    all_gather x1, waiting for transfers between devices: 16.7 us -> 28.8 us  [on_device(): lax.all_gather(output_gate_matrix, 'fs', axis=0, tiled=True)]
    all_gather x1, waiting for transfers between devices: 28.8 us -> 18.8 us  [on_device(): lax.all_gather(merge_weight, 'fs', axis=1, tiled=True)]
  transfers between devices with their start and end apart: 12 -> 14, of which waited for: 12 -> 13; matrix products, arithmetic and copies ran while one was open for 6% -> 8% of each run, Pallas kernels for 0% -> 0%
where the time goes in v1:
time: 529 us
  waiting for transfers between devices  449 us (85%)
  matrix products  33.1 us (6%)
  local copies, waits for them, and re-layouts  17.1 us (3%)
  between operations  13.6 us (3%)
  other arithmetic  9.76 us (2%)
  starting transfers between devices  5.77 us (1%)
    all_gather x1, waiting for transfers between devices, on_device(): lax.all_gather(up_weight, 'fs', axis=0, tiled=True)  91.3 us
    ppermute x2, waiting for transfers between devices, collect(): earlier.append(lax.ppermute(earlier[-1], axis, up))  88.6 us
    ppermute x1, waiting for transfers between devices, collect(): later.append(lax.ppermute(later[-1], axis, down))  49.1 us
    all_gather x1, waiting for transfers between devices, on_device(): lax.all_gather(output_gate_matrix, 'fs', axis=0, tiled=True)  28.8 us
    all_gather x1, waiting for transfers between devices, on_device(): lax.all_gather(value_weight, 'fs', axis=0, tiled=True)  27.8 us
    reduce_scatter x1, waiting for transfers between devices, on_device(): lax.psum_scatter(merge_term.astype(jnp.bfloat16), 'tp', scatter_dimension...  27.5 us
    all_gather x1, waiting for transfers between devices, on_device(): lax.all_gather(key_weight, 'fs', axis=0, tiled=True)  26.7 us
    reduce_scatter x1, waiting for transfers between devices, on_device(): lax.psum_scatter(down_term.astype(jnp.bfloat16), 'tp', scatter_dimension=...  26.5 us
  transfers between devices with their start and end apart: 14, of which 13 were waited for; matrix products, arithmetic and copies ran while one was open for 8% of the time, Pallas kernels for 0%

profile of v1, /device:TPU:0, one launch (start us, length us, event | category | flops | bytes accessed | tf_op | source)
XLA Modules:
  0.0 528.9 jit_solution(12681799811731377722)
XLA Ops:
  11.9 19.3 %all-gather.10.cloned.1.call-done = bf16[1,384,2048]{2,1,0:T(8,128)(2,1)} async-done(((bf16[1,384,512]{2,1,0:T(8,128)(2,1)}), bf16[1,384,2048]{2,1,0:T(8,128)(2,1)}) %all-gather.10.cloned.1.call-update) | async-done | bytes 1572880 | tf_op jit(solution)/shard_map/all_gather | solution.py:147
  31.3 1.8 fusion.5
  33.1 27.8 %all-gather.14.cloned.1.call-done = bf16[2048,256]{1,0:T(8,128)(2,1)} async-done(((bf16[512,256]{1,0:T(8,128)(2,1)}), bf16[2048,256]{1,0:T(8,128)(2,1)}) %all-gather.14.cloned.1.call-update) | async-done | bytes 1048592 | tf_op jit(solution)/shard_map/all_gather | solution.py:153
  60.9 2.3 convolution_convert_fusion.3
  63.6 26.2 %all-gather.16.cloned.1.call-done = bf16[2048,256]{1,0:T(8,128)(2,1)} async-done(((bf16[512,256]{1,0:T(8,128)(2,1)}), bf16[2048,256]{1,0:T(8,128)(2,1)}) %all-gather.16.cloned.1.call-update) | async-done | bytes 1048592 | tf_op jit(solution)/shard_map/all_gather | solution.py:151
  89.8 2.1 convolution_convert_fusion.2
  92.0 26.7 %all-gather.18.cloned.1.call-done = bf16[2048,256]{1,0:T(8,128)(2,1)} async-done(((bf16[512,256]{1,0:T(8,128)(2,1)}), bf16[2048,256]{1,0:T(8,128)(2,1)}) %all-gather.18.cloned.1.call-update) | async-done | bytes 1048592 | tf_op jit(solution)/shard_map/all_gather | solution.py:152
  118.6 2.1 convolution_convert_fusion.1
  125.1 1.4 convolution_multiply_fusion.1
  128.7 18.8 %all-gather.20.cloned.1.call-done = bf16[256,2048]{1,0:T(8,128)(2,1)} async-done(((bf16[256,512]{1,0:T(8,128)(2,1)}), bf16[256,2048]{1,0:T(8,128)(2,1)}) %all-gather.20.cloned.1.call-update) | async-done | bytes 1048592 | tf_op jit(solution)/shard_map/all_gather | solution.py:170
  147.5 28.8 %all-gather.12.cloned.1.call-done = bf16[2048,256]{1,0:T(8,128)(2,1)} async-done(((bf16[512,256]{1,0:T(8,128)(2,1)}), bf16[2048,256]{1,0:T(8,128)(2,1)}) %all-gather.12.cloned.1.call-update) | async-done | bytes 1048592 | tf_op jit(solution)/shard_map/all_gather | solution.py:154
  176.3 4.6 convolution_convert_fusion
  180.9 27.5 %reduce-scatter.3.cloned.1.call-done = bf16[384,512]{1,0:T(8,128)(2,1)} async-done(((bf16[384,2048]{1,0:T(8,128)(2,1)}), bf16[384,512]{1,0:T(8,128)(2,1)}) %reduce-scatter.3.cloned.1.call-update) | async-done | bytes 393232 | tf_op jit(solution)/shard_map/reduce_scatter | solution.py:173
  208.4 1.8 fusion.18
  211.7 1.6 collective-permute-start
  213.2 30.8 %collective-permute-done = bf16[1280,512]{1,0:T(8,128)(2,1)S(1)} collective-permute-done((bf16[1280,512]{1,0:T(8,128)(2,1)S(1)}, bf16[1280,512]{1,0:T(8,128)(2,1)S(1)}, u32[]{:S(2)}, u32[]{:S(2)}) %collective-permute-start) | collective-permute-done | bytes 1310752 | tf_op jit(solution)/shard_map/ppermute | solution.py:19
  244.1 3.7 collective-permute-start.2
  247.8 57.8 %collective-permute-done.1 = bf16[1280,512]{1,0:T(8,128)(2,1)} collective-permute-done((bf16[1280,512]{1,0:T(8,128)(2,1)S(1)}, bf16[1280,512]{1,0:T(8,128)(2,1)}, u32[]{:S(2)}, u32[]{:S(2)}) %collective-permute-start.1) | collective-permute-done | bytes 1310752 | tf_op jit(solution)/shard_map/ppermute | solution.py:19
  305.6 2.5 constant_dynamic-update-slice_fusion.9
  309.4 1.3 constant_dynamic-update-slice_fusion.7
  310.6 49.1 %collective-permute-done.2 = bf16[1280,512]{1,0:T(8,128)(2,1)} collective-permute-done((bf16[1280,512]{1,0:T(8,128)(2,1)S(1)}, bf16[1280,512]{1,0:T(8,128)(2,1)}, u32[]{:S(2)}, u32[]{:S(2)}) %collective-permute-start.2) | collective-permute-done | bytes 1310752 | tf_op jit(solution)/shard_map/ppermute | solution.py:21
  359.7 2.6 constant_dynamic-update-slice_fusion.6
  362.3 2.6 constant_dynamic-update-slice_fusion.5
  364.9 1.3 constant_dynamic-update-slice_fusion.4
  367.3 2.5 constant_dynamic-update-slice_fusion.2
  369.8 1.8 fusion.2
  371.6 13.9 %all-gather.24.cloned.1.call-done = bf16[2048,1280]{1,0:T(8,128)(2,1)} async-done(((bf16[512,1280]{1,0:T(8,128)(2,1)}), bf16[2048,1280]{1,0:T(8,128)(2,1)}) %all-gather.24.cloned.1.call-update) | async-done | bytes 5242896 | tf_op jit(solution)/shard_map/all_gather | solution.py:182
  385.5 6.5 %fusion.21 = f32[384,1280]{1,0:T(8,128)} fusion(bf16[2048,1280]{1,0:T(8,128)(2,1)} %all-gather.24.cloned.1.call-done, bf16[384,2048]{1,0:T(8,128)(2,1)} %all-gather.22.cloned.1.call-done, f32[2048]{0:T(1024)S(1)} %copy-done.7, f32[384]{0:T(512)S(1)} %add_rsqrt_fusion), kind=kOutput, calls=%fused_computation.39 | convolution fusion | flops 2016411648 | bytes 8791552 | tf_op jit(solution)/shard_map/dot_general | solution.py:185
  392.1 91.3 %all-gather.26.cloned.1.call-done = bf16[2048,1280]{1,0:T(8,128)(2,1)} async-done(((bf16[512,1280]{1,0:T(8,128)(2,1)}), bf16[2048,1280]{1,0:T(8,128)(2,1)}) %all-gather.26.cloned.1.call-update) | async-done | bytes 5242896 | tf_op jit(solution)/shard_map/all_gather | solution.py:183
  483.4 10.7 %fusion.9 = bf16[384,2048]{1,0:T(8,128)(2,1)} fusion(bf16[1280,4096]{1,0:T(8,128)(2,1)} %constant_dynamic-update-slice_fusion.2, s32[]{:T(128)S(6)} %select_n.33, bf16[2048,1280]{1,0:T(8,128)(2,1)} %all-gather.26.cloned.1.call-done, f32[384,1280]{1,0:T(8,128)} %fusion.21, bf16[384,2048]{1,0:T(8,128)(2,1)S(1)} %copy-done.4, f32[2048]{0:T(1024)S(1)} %copy-done.7, ...), kind=kOutput, calls=%fused_computation.18 | convolution fusion | flops 4033413120 | bytes 15607300 | tf_op jit(solution)/shard_map/dot_general | solution.py:188
  494.1 26.5 %reduce-scatter.5.cloned.1.call-done = bf16[384,512]{1,0:T(8,128)(2,1)} async-done(((bf16[384,2048]{1,0:T(8,128)(2,1)}), bf16[384,512]{1,0:T(8,128)(2,1)}) %reduce-scatter.5.cloned.1.call-update) | async-done | bytes 393232 | tf_op jit(solution)/shard_map/reduce_scatter | solution.py:189
  520.6 1.8 fusion.23
  (98 shorter events, 16.6 us)
Async XLA Ops:
  6.5 54.3 %copy-start.6 = (f32[2048]{0:T(1024)S(1)}, f32[2048]{0:T(1024)}, u32[]{:S(2)}) copy-start(f32[2048]{0:T(1024)} %param.18) | copy-start | bytes 24580
  6.5 24.7 %all-gather.10.cloned.1.call-start = ((), (), s32[]{:S(2)}) async-start(), calls=%async_computation.2 | async-start | bytes 1966080 | tf_op jit(solution)/shard_map/all_gather | solution.py:147
  7.3 53.6 %all-gather.14.cloned.1.call-start = ((), (), s32[]{:S(2)}) async-start(), calls=%async_computation.4 | async-start | bytes 1310720 | tf_op jit(solution)/shard_map/all_gather | solution.py:153
  8.0 81.8 %all-gather.16.cloned.1.call-start = ((), (), s32[]{:S(2)}) async-start(), calls=%async_computation.5 | async-start | bytes 1310720 | tf_op jit(solution)/shard_map/all_gather | solution.py:151
  8.7 109.9 %all-gather.18.cloned.1.call-start = ((), (), s32[]{:S(2)}) async-start(), calls=%async_computation.6 | async-start | bytes 1310720 | tf_op jit(solution)/shard_map/all_gather | solution.py:152
  9.3 138.1 %all-gather.20.cloned.1.call-start = ((), (), s32[]{:S(2)}) async-start(), calls=%async_computation.7 | async-start | bytes 1310720 | tf_op jit(solution)/shard_map/all_gather | solution.py:170
  9.9 166.4 %all-gather.12.cloned.1.call-start = ((), (), s32[]{:S(2)}) async-start(), calls=%async_computation.3 | async-start | bytes 1310720 | tf_op jit(solution)/shard_map/all_gather | solution.py:154
  10.5 197.9 %reduce-scatter.3.cloned.1.call-start = ((), (), s32[]{:S(2)}) async-start(), calls=%async_computation.8 | async-start | bytes 1966080 | tf_op jit(solution)/shard_map/reduce_scatter | solution.py:173
  33.1 56.8 %copy-start.2 = (bf16[1,384,2048]{2,1,0:T(8,128)(2,1)S(1)}, bf16[1,384,2048]{2,1,0:T(8,128)(2,1)}, u32[]{:S(2)}) copy-start(bf16[1,384,2048]{2,1,0:T(8,128)(2,1)} %all-gather.10.cloned.1.call-done) | copy-start | bytes 4718596
  126.5 49.8 %copy-start.3 = (bf16[1,384,2048]{2,1,0:T(8,128)(2,1)S(1)}, bf16[1,384,2048]{2,1,0:T(8,128)(2,1)}, u32[]{:S(2)}) copy-start(bf16[1,384,2048]{2,1,0:T(8,128)(2,1)} %all-gather.10.cloned.1.call-done) | copy-start | bytes 4718596
  128.7 79.7 %copy-start.5 = (bf16[1,384,512]{2,1,0:T(8,128)(2,1)S(1)}, bf16[1,384,512]{2,1,0:T(8,128)(2,1)}, u32[]{:S(2)}) copy-start(bf16[1,384,512]{2,1,0:T(8,128)(2,1)} %param.17) | copy-start | bytes 1179652
  180.9 30.8 %copy-start = (bf16[1280,512]{1,0:T(8,128)(2,1)S(1)}, bf16[1280,512]{1,0:T(8,128)(2,1)}, u32[]{:S(2)}) copy-start(bf16[1280,512]{1,0:T(8,128)(2,1)} %param.29) | copy-start | bytes 3932164
  180.9 188.9 %all-gather.22.cloned.1.call-start = ((), (), s32[]{:S(2)}) async-start(), calls=%async_computation.9 | async-start | bytes 1966080 | tf_op jit(solution)/shard_map/all_gather | solution.py:179
  210.3 175.2 %all-gather.24.cloned.1.call-start = ((), (), s32[]{:S(2)}) async-start(), calls=%async_computation.10 | async-start | bytes 6553600 | tf_op jit(solution)/shard_map/all_gather | solution.py:182
  211.0 272.4 %all-gather.26.cloned.1.call-start = ((), (), s32[]{:S(2)}) async-start(), calls=%async_computation.11 | async-start | bytes 6553600 | tf_op jit(solution)/shard_map/all_gather | solution.py:183
  211.6 308.9 %reduce-scatter.5.cloned.1.call-start = ((), (), s32[]{:S(2)}) async-start(), calls=%async_computation.12 | async-start | bytes 1966080 | tf_op jit(solution)/shard_map/reduce_scatter | solution.py:189
  211.7 32.3 %collective-permute-start = (bf16[1280,512]{1,0:T(8,128)(2,1)S(1)}, bf16[1280,512]{1,0:T(8,128)(2,1)S(1)}, u32[]{:S(2)}, u32[]{:S(2)}) collective-permute-start(bf16[1280,512]{1,0:T(8,128)(2,1)S(1)} %copy-done), channel_id=1, source_target_pairs={{0,4},{4,8},{8,12},{12,0},{1,5},{5,9},{9,13},{13,1},{2,6},{6,10},{... | collective-permute-start | bytes 3932168 | tf_op jit(solution)/shard_map/ppermute | solution.py:19
  244.0 61.6 %collective-permute-start.1 = (bf16[1280,512]{1,0:T(8,128)(2,1)S(1)}, bf16[1280,512]{1,0:T(8,128)(2,1)}, u32[]{:S(2)}, u32[]{:S(2)}) collective-permute-start(bf16[1280,512]{1,0:T(8,128)(2,1)S(1)} %collective-permute-done), channel_id=1, source_target_pairs={{0,4},{4,8},{8,12},{12,0},{1,5},{5,9},{9,13},{13,1},{2,6},{6,10},{... | collective-permute-start | bytes 3932168 | tf_op jit(solution)/shard_map/ppermute | solution.py:19
  244.1 115.6 %collective-permute-start.2 = (bf16[1280,512]{1,0:T(8,128)(2,1)S(1)}, bf16[1280,512]{1,0:T(8,128)(2,1)}, u32[]{:S(2)}, u32[]{:S(2)}) collective-permute-start(bf16[1280,512]{1,0:T(8,128)(2,1)S(1)} %copy-done), channel_id=1, source_target_pairs={{0,12},{4,0},{8,4},{12,8},{1,13},{5,1},{9,5},{13,9},{2,14},{6,2},{... | collective-permute-start | bytes 3932168 | tf_op jit(solution)/shard_map/ppermute | solution.py:21
  366.1 19.4 %copy-start.7 = (f32[2048]{0:T(1024)S(1)}, f32[2048]{0:T(1024)}, u32[]{:S(2)}) copy-start(f32[2048]{0:T(1024)} %param.26) | copy-start | bytes 24580
  371.6 111.8 %copy-start.4 = (bf16[384,2048]{1,0:T(8,128)(2,1)S(1)}, bf16[384,2048]{1,0:T(8,128)(2,1)}, u32[]{:S(2)}) copy-start(bf16[384,2048]{1,0:T(8,128)(2,1)} %all-gather.22.cloned.1.call-done) | copy-start | bytes 4718596
  392.1 128.5 %copy-start.1 = (bf16[384,512]{1,0:T(8,128)(2,1)S(1)}, bf16[384,512]{1,0:T(8,128)(2,1)}, u32[]{:S(2)}) copy-start(bf16[384,512]{1,0:T(8,128)(2,1)} %fusion.18) | copy-start | bytes 1179652
Sparse Core Ops, SparseCore 0:
  8.9 22.3 all-gather.9
  32.8 27.9 all-gather.13
  62.4 27.3 all-gather.15
  91.3 27.3 all-gather.17
  120.1 27.3 all-gather.19
  148.9 27.3 all-gather.11
  181.0 27.3 reduce-scatter.2
  210.4 19.6 all-gather.21
  231.7 153.8 all-gather.23
  386.9 96.3 all-gather.25
  494.2 26.3 reduce-scatter.4
